TPU v7x, 512 devices: a 4x2x32 block of a 4x8x32 slice. The times are simulated.
512 devices in a mesh: grp: 2 (over y), sp: 32 (over z), tp: 8 (over x, core).
Axes of the slice: x: 4, y: 2, z: 32, core: 2. Of those that a mesh axis runs over, the one named last changes fastest.
The devices are a block of a 4x8x32 slice.
Arguments:
- tokens: bfloat16 [32768, 2048], P(('grp', 'sp')), parts along dimension 0, may hold values from -6 to 6
- fresh_token_input: bfloat16 [4096], P('grp'), parts along dimension 0, may hold values from -6 to 6
- value_matrix: bfloat16 [2048, 2048], P(None, 'tp'), may hold values from -0.125 to 0.125
- write_matrix: bfloat16 [2048, 1024], P(None, 'tp'), may hold values from -0.125 to 0.125
- read_matrix: bfloat16 [2048, 1024], P(None, 'tp'), may hold values from -0.125 to 0.125
- gate_matrix: bfloat16 [2048, 2048], P(None, 'tp'), may hold values from -0.125 to 0.125
- step_matrix: bfloat16 [2048, 32], replicated, may hold values from -0.125 to 0.125
- value_filter_taps: bfloat16 [4, 2048], replicated, may hold values from -3 to 3
- write_filter_taps: bfloat16 [4, 1024], replicated, may hold values from -3 to 3
- read_filter_taps: bfloat16 [4, 1024], replicated, may hold values from -3 to 3
- head_log_decay: float32 [32], replicated
- step_offset_bias: float32 [32], replicated, may hold values from -3.5 to -2.5
- decay_spike: float32 [32768, 32], P(('grp', 'sp'), 'tp'), parts along dimension 0, may hold values from -3 to 0, as said below
- bypass_scale: float32 [32], replicated, may hold values from 0.5 to 2
- group_norm_scale: float32 [2048], replicated, may hold values from 0.1 to 1.9
Outputs:
- prompt_out: bfloat16 [32768, 2048], P(('grp', 'sp'), 'tp'), parts along dimension 0
- state_cache: bfloat16 [256, 2048], P(('grp', 'sp'), 'tp'), parts along dimension 0
- step_out: bfloat16 [128, 32], P(('grp', 'tp'), 'sp'), parts along dimension 0
There are 2 independent parts, one for each index of `grp`. A program takes and returns all parts, laid end to end along the dimension named above; an argument that names none is the same for every part. Nothing has to cross between parts.
Inputs may be any that keep to these rules, and one draw needn't show every extreme that they name: `decay_spike`: never positive.
All inputs are finite; a program needn't handle non-finite values.
Results may differ from a plain program's by a relative error of at most 0.023.
Values may be sent and summed in bfloat16 or wider, within the bound.
No kernel may reach another device: no remote copies, remote signals or barrier semaphores. Data moves between devices by JAX's collectives and lax.ppermute only.
A program may use at most 64 MiB of HBM per device.

v0:
```python
import jax
import jax.numpy as jnp
from jax import lax
from jax.sharding import PartitionSpec as P

HEAD = 64
STATE = 128
CONV = 4
BLOCK = 128
epsilon = 1e-06


def passed_along(block, axis, distance):
    devices = range(lax.axis_size(axis))
    route = [(i - distance, i) for i in devices if i - distance in devices]
    return lax.ppermute(block, axis, route)


def from_root(value, axis, source):
    kept = jnp.where(lax.axis_index(axis) == source, value, 0).astype(value.dtype)
    return lax.psum(kept, axis)


def in_order(pieces, dim):
    dims = list(pieces.shape[1:])
    dims[dim] *= pieces.shape[0]
    return jnp.moveaxis(pieces, 0, dim).reshape(dims)


def from_everyone(value, axis):
    peers = lax.axis_size(axis)
    return lax.all_to_all(
        jnp.broadcast_to(value[None], (peers, *value.shape)), axis, 0, 0, tiled=True
    )


def gather_directly(value, axis, dim):
    return in_order(from_everyone(value, axis), dim)


def taken_together(value, axis):
    everything = from_everyone(value, axis)
    return jnp.sum(everything, axis=0)


def project(operand, weights):
    return jnp.dot(operand, weights, preferred_element_type=jnp.float32).astype(jnp.bfloat16)


def apply_taps(previous, current, tap_weights):
    joined = jnp.concatenate([previous, current], axis=0).astype(jnp.float32)
    length = current.shape[0]
    summed = jnp.zeros(current.shape, jnp.float32)
    for offset in range(CONV):
        summed = summed + tap_weights[offset].astype(jnp.float32) * joined[offset : offset + length]
    return summed


def group_norm(gated_rows, groups):
    shaped = gated_rows.reshape(gated_rows.shape[:-1] + (groups, -1))
    normed = shaped * lax.rsqrt(jnp.mean(shaped * shaped, axis=-1, keepdims=True) + epsilon)
    return normed.reshape(gated_rows.shape)


def read_new(cached, stored_portion, read_part, new_decay, step_now, value_now):
    states = cached.astype(jnp.float32).reshape((cached.shape[0],) + value_now.shape)
    updated = (
        new_decay[None, :, :, None] * states
        + step_now[None, :, :, None] * stored_portion.T[:, :, None, None] * value_now[None]
    )
    return jnp.einsum("gn,ngep->gep", read_part, updated)


def on_device(
    tokens,
    fresh_token_input,
    value_matrix,
    write_matrix,
    read_matrix,
    gate_matrix,
    step_matrix,
    value_filter_taps,
    write_filter_taps,
    read_filter_taps,
    head_log_decay,
    step_offset_bias,
    decay_spike,
    bypass_scale,
    group_norm_scale,
):
    head_rank = lax.axis_index("tp")
    sequence_rank = lax.axis_index("sp")
    sequence_count = lax.axis_size("sp")
    channels = value_matrix.shape[1]
    head_count = channels // HEAD
    map_width = write_matrix.shape[1]
    group_count = map_width // STATE
    per_group = head_count // group_count
    row_count = tokens.shape[0]
    head_start = head_rank * head_count
    local_count = STATE // sequence_count
    own_step = lax.dynamic_slice_in_dim(step_matrix, head_start, head_count, 1)
    own_value_taps = lax.dynamic_slice_in_dim(value_filter_taps, head_rank * channels, channels, 1)
    own_write_taps = lax.dynamic_slice_in_dim(
        write_filter_taps, head_rank * map_width, map_width, 1
    )
    own_read_taps = lax.dynamic_slice_in_dim(read_filter_taps, head_rank * map_width, map_width, 1)
    head_decay_rates = jnp.exp(lax.dynamic_slice_in_dim(head_log_decay, head_start, head_count, 0))
    own_bias = lax.dynamic_slice_in_dim(step_offset_bias, head_start, head_count, 0)
    own_skip = lax.dynamic_slice_in_dim(bypass_scale, head_start, head_count, 0)
    own_gain = lax.dynamic_slice_in_dim(group_norm_scale, head_rank * channels, channels, 0)
    value_rows = project(tokens, value_matrix)
    write_rows = project(tokens, write_matrix)
    read_rows = project(tokens, read_matrix)
    gate_rows = project(tokens, gate_matrix)
    step_raw = jnp.dot(tokens, own_step, preferred_element_type=jnp.float32)
    edge = row_count - (CONV - 1)
    tail_rows = (value_rows[edge:], write_rows[edge:], read_rows[edge:])
    before = passed_along((tail_rows[0], tail_rows[1], tail_rows[2]), "sp", 1)
    ending = (
        from_root(tail_rows[0], "sp", sequence_count - 1),
        from_root(tail_rows[1], "sp", sequence_count - 1),
        from_root(tail_rows[2], "sp", sequence_count - 1),
    )
    values = jax.nn.silu(apply_taps(before[0], value_rows, own_value_taps)).astype(jnp.bfloat16)
    writes = jax.nn.silu(apply_taps(before[1], write_rows, own_write_taps)).astype(jnp.bfloat16)
    reads = jax.nn.silu(apply_taps(before[2], read_rows, own_read_taps)).astype(jnp.bfloat16)
    step_length = jax.nn.softplus(step_raw + own_bias)
    log_decay_value = decay_spike - step_length * head_decay_rates
    blocks = row_count // BLOCK
    block_values = values.reshape(blocks, BLOCK, group_count, per_group, HEAD)
    block_writes = writes.reshape(blocks, BLOCK, group_count, STATE)
    block_reads = reads.reshape(blocks, BLOCK, group_count, STATE)
    block_steps = step_length.reshape(blocks, BLOCK, group_count, per_group)
    cumulative = jnp.cumsum(log_decay_value.reshape(blocks, BLOCK, group_count, per_group), axis=1)
    block_end = cumulative[:, -1]
    scaled = (
        (jnp.exp(block_end[:, None] - cumulative) * block_steps)[..., None]
        * block_values.astype(jnp.float32)
    ).astype(jnp.bfloat16)
    block_states = jnp.einsum(
        "bsgn,bsgep->bngep", block_writes, scaled, preferred_element_type=jnp.float32
    )
    running = jnp.zeros((STATE, group_count, per_group, HEAD), jnp.float32)
    inside = []
    for block_index in range(blocks):
        inside.append(running)
        running = (
            jnp.exp(block_end[block_index])[None, :, :, None] * running + block_states[block_index]
        )
    local_states = jnp.stack(inside)
    shard_fading_factor = jnp.sum(block_end, axis=0)
    before_block = jnp.cumsum(block_end, axis=0) - block_end
    decay_table = gather_directly(shard_fading_factor[None], "sp", 0)
    inclusive = jnp.cumsum(decay_table, axis=0)
    exclusive = inclusive - decay_table
    total_decay = inclusive[-1]
    row_pieces = lax.all_to_all(running[None], "sp", split_axis=1, concat_axis=0, tiled=True)
    ranks = jnp.arange(sequence_count)
    below = (ranks[None, :] < ranks[:, None])[:, :, None, None]
    prefix_weight = jnp.exp(jnp.where(below, exclusive[:, None] - inclusive[None, :], -jnp.inf))
    prefix_rows = jnp.einsum("jkge,kngep->jngep", prefix_weight, row_pieces)
    final_weight = jnp.exp(total_decay[None] - inclusive)
    final_rows = jnp.einsum("kge,kngep->ngep", final_weight, row_pieces)
    earlier_state = lax.all_to_all(prefix_rows, "sp", split_axis=0, concat_axis=1, tiled=True)[0]
    scores = jnp.einsum(
        "blgn,bsgn->bgls", block_reads, block_writes, preferred_element_type=jnp.float32
    )
    cum_heads = jnp.transpose(cumulative, (0, 2, 3, 1))
    decay_gaps = cum_heads[..., :, None] - cum_heads[..., None, :]
    step_heads = jnp.transpose(block_steps, (0, 2, 3, 1))
    causal = jnp.tril(jnp.ones((BLOCK, BLOCK), bool))
    mixing = (
        scores[:, :, None]
        * jnp.exp(jnp.where(causal, decay_gaps, -jnp.inf))
        * step_heads[..., None, :]
    ).astype(jnp.bfloat16)
    inner_part = jnp.einsum(
        "bgels,bsgep->blgep", mixing, block_values, preferred_element_type=jnp.float32
    )
    entering = jnp.exp(before_block)[:, None, :, :, None] * earlier_state[None] + local_states
    carried_part = jnp.exp(cumulative)[..., None] * jnp.einsum(
        "blgn,bngep->blgep", block_reads.astype(jnp.float32), entering
    )
    mixed_rows = (inner_part + carried_part).reshape(row_count, head_count, HEAD) + own_skip[
        None, :, None
    ] * values.astype(jnp.float32).reshape(row_count, head_count, HEAD)
    gated_rows = mixed_rows.reshape(row_count, channels) * jax.nn.silu(
        gate_rows.astype(jnp.float32)
    )
    prompt_out = (group_norm(gated_rows, group_count) * own_gain).astype(jnp.bfloat16)
    new_row = fresh_token_input[None]
    new_value = project(new_row, value_matrix)
    new_write = project(new_row, write_matrix)
    new_read = project(new_row, read_matrix)
    new_gate = project(new_row, gate_matrix)
    new_step = jax.nn.softplus(
        jnp.dot(new_row, own_step, preferred_element_type=jnp.float32)[0] + own_bias
    )
    new_values = jax.nn.silu(apply_taps(ending[0], new_value, own_value_taps)).astype(jnp.bfloat16)
    latest_stores = jax.nn.silu(apply_taps(ending[1], new_write, own_write_taps)).astype(
        jnp.bfloat16
    )
    new_reads = jax.nn.silu(apply_taps(ending[2], new_read, own_read_taps)).astype(jnp.bfloat16)
    value_now = new_values.astype(jnp.float32).reshape(group_count, per_group, HEAD)
    write_now = latest_stores.astype(jnp.float32)
    read_now = new_reads.astype(jnp.float32)
    new_decay = jnp.exp(-new_step * head_decay_rates).reshape(group_count, per_group)
    step_now = new_step.reshape(group_count, per_group)
    row_start = sequence_rank * local_count
    cache_rows = final_rows.reshape(local_count, channels).astype(jnp.bfloat16)
    stored_portion = lax.dynamic_slice_in_dim(write_now, row_start, local_count, 1)
    read_part = lax.dynamic_slice_in_dim(read_now, row_start, local_count, 1)
    partial_value = read_new(cache_rows, stored_portion, read_part, new_decay, step_now, value_now)
    reading = taken_together(partial_value, "sp")
    new_mixed = reading + own_skip.reshape(group_count, per_group)[:, :, None] * value_now
    new_gated = new_mixed.reshape(1, channels) * jax.nn.silu(new_gate.astype(jnp.float32))
    step_whole = (group_norm(new_gated, group_count) * own_gain).astype(jnp.bfloat16)[0]
    step_table = step_whole.reshape(channels // sequence_count, sequence_count)
    step_out = lax.dynamic_slice_in_dim(step_table, sequence_rank, 1, 1)
    return (prompt_out, cache_rows, step_out)


def solution(mesh):
    placed = (
        P(("grp", "sp"), None),
        P("grp"),
        P(None, "tp"),
        P(None, "tp"),
        P(None, "tp"),
        P(None, "tp"),
        P(),
        P(),
        P(),
        P(),
        P(),
        P(),
        P(("grp", "sp"), "tp"),
        P(),
        P(),
    )
    return jax.shard_map(
        on_device,
        mesh=mesh,
        in_specs=placed,
        out_specs=(P(("grp", "sp"), "tp"), P(("grp", "sp"), "tp"), P(("grp", "tp"), "sp")),
        check_vma=False,
    )
```

profile of v0, /device:TPU:46, one launch (start us, length us, event | category | flops | bytes accessed | tf_op | source)
XLA Modules:
  0.0 264.0 jit_solution(4816721934194735863)
XLA Ops:
  0.7 1.6 copy-done
  2.2 1.8 convolution_convert_fusion.2
  4.6 5.3 %collective-permute-start.2 = (bf16[3,128]{1,0:T(4,128)(2,1)}, bf16[3,128]{1,0:T(4,128)(2,1)}, u32[]{:S(2)}, u32[]{:S(2)}) collective-permute-start(bf16[3,128]{1,0:T(4,128)(2,1)} %get-tuple-element.46), channel_id=1, source_target_pairs={{0,8},{8,16},{16,24},{24,32},{32,40},{40,48},{48,56},{56,64},{64,7... | collective-permute-start | bytes 2312 | tf_op jit(solution)/shard_map/ppermute | solution.py:16
  9.9 0.7 convolution_convert_fusion.3
  11.3 4.7 %collective-permute-start.1 = (bf16[3,128]{1,0:T(4,128)(2,1)}, bf16[3,128]{1,0:T(4,128)(2,1)}, u32[]{:S(2)}, u32[]{:S(2)}) collective-permute-start(bf16[3,128]{1,0:T(4,128)(2,1)} %get-tuple-element.44), channel_id=1, source_target_pairs={{0,8},{8,16},{16,24},{24,32},{32,40},{40,48},{48,56},{56,64},{64,7... | collective-permute-start | bytes 2312 | tf_op jit(solution)/shard_map/ppermute | solution.py:16
  16.1 1.5 multiply_exponential_fusion
  17.5 1.4 multiply_subtract_fusion
  20.6 43.0 %all-to-all-start.1 = ((f32[32,1,1,4]{3,2,1,0:T(1,128)}), f32[32,1,1,4]{3,2,1,0:T(1,128)}, u32[]{:S(2)}, u32[]{:S(2)}) async-start(f32[32,1,1,4]{3,2,1,0:T(1,128)} %broadcast_in_dim.36), calls=%async_computation.1 | async-start | bytes 32768 | tf_op jit(solution)/shard_map/all_to_all | solution.py:32
  63.6 1.9 convolution_convert_fusion.1
  65.5 0.7 copy-done.6
  66.8 3.8 %collective-permute-start = (bf16[3,256]{1,0:T(4,128)(2,1)}, bf16[3,256]{1,0:T(4,128)(2,1)}, u32[]{:S(2)}, u32[]{:S(2)}) collective-permute-start(bf16[3,256]{1,0:T(4,128)(2,1)} %get-tuple-element.42), channel_id=1, source_target_pairs={{0,8},{8,16},{16,24},{24,32},{32,40},{40,48},{48,56},{56,64},{64,7... | collective-permute-start | bytes 4616 | tf_op jit(solution)/shard_map/ppermute | solution.py:16
  71.2 0.7 fusion.5
  72.2 1.5 fusion.89
  75.0 0.7 dynamic_slice.39
  75.8 0.7 constant_dynamic-slice_fusion.4
  76.5 2.1 fusion.90
  79.9 56.4 %all-reduce = (bf16[3,256]{1,0:T(4,128)(2,1)S(1)}, bf16[3,128]{1,0:T(4,128)(2,1)S(1)}, bf16[3,128]{1,0:T(4,128)(2,1)S(1)}) all-reduce(bf16[3,256]{1,0:T(4,128)(2,1)S(1)} %copy-done.13, bf16[3,128]{1,0:T(4,128)(2,1)S(1)} %copy-done.18, bf16[3,128]{1,0:T(4,128)(2,1)S(1)} %copy-done.19), channel_id=1, replica_groups=mesh['grp'=2,'sp'=32,'tp'=8] {'sp'}, use_global_device_ids=true, to_apply=%region_7.8 | all-reduce | flops 1536 | bytes 6144 | tf_op jit(solution)/shard_map/psum | solution.py:21
  137.6 2.2 fusion.85
  140.4 0.7 mul.534
  141.7 0.7 copy.147
  143.1 0.7 maximum_convert_fusion.1
  143.9 0.7 maximum_convert_fusion.2
  144.8 0.9 fusion.88
  145.7 0.7 maximum_convert_fusion
  147.5 0.8 slice_add_fusion
  148.4 0.7 reshape.495
  149.1 19.8 %all-to-all-start = ((bf16[32,2,512]{2,1,0:T(2,128)(2,1)}), bf16[32,2,512]{2,1,0:T(2,128)(2,1)S(1)}, u32[]{:S(2)}, u32[]{:S(2)}) async-start(bf16[32,2,512]{2,1,0:T(2,128)(2,1)} %reshape.495), calls=%async_computation | async-start | bytes 131072 | tf_op jit(solution)/shard_map/all_to_all | solution.py:158
  169.0 0.8 fusion.48
  169.8 0.8 copy.162
  170.7 22.1 %all-to-all-done = bf16[32,2,512]{2,1,0:T(2,128)(2,1)S(1)} async-done(((bf16[32,2,512]{2,1,0:T(2,128)(2,1)}), bf16[32,2,512]{2,1,0:T(2,128)(2,1)S(1)}, u32[]{:S(2)}, u32[]{:S(2)}) %all-to-all-start) | async-done | bytes 65568 | tf_op jit(solution)/shard_map/all_to_all | solution.py:158
  193.4 0.7 reshape.499
  194.1 5.3 %all-to-all-start.3 = ((f32[32,1,256]{2,1,0:T(1,128)}), f32[32,1,256]{2,1,0:T(1,128)}, u32[]{:S(2)}, u32[]{:S(2)}) async-start(f32[32,1,256]{2,1,0:T(1,128)} %reshape.499), calls=%async_computation.3 | async-start | bytes 65536 | tf_op jit(solution)/shard_map/all_to_all | solution.py:32
  199.9 0.9 reshape.497
  200.8 21.1 %all-to-all-done.3 = f32[32,1,256]{2,1,0:T(1,128)} async-done(((f32[32,1,256]{2,1,0:T(1,128)}), f32[32,1,256]{2,1,0:T(1,128)}, u32[]{:S(2)}, u32[]{:S(2)}) %all-to-all-start.3) | async-done | bytes 32800 | tf_op jit(solution)/shard_map/all_to_all | solution.py:32
  221.8 5.0 %all-to-all-start.2 = ((f32[32,1,1024]{2,1,0:T(1,128)}), f32[32,1,1024]{2,1,0:T(1,128)S(1)}, u32[]{:S(2)}, u32[]{:S(2)}) async-start(f32[32,1,1024]{2,1,0:T(1,128)} %reshape.497), calls=%async_computation.2 | async-start | bytes 262144 | tf_op jit(solution)/shard_map/all_to_all | solution.py:165
  226.8 1.3 fusion.39
  228.1 1.6 fusion.52
  230.9 1.5 reduce.19
  232.6 1.3 multiply_reduce_fusion.1
  234.6 1.3 multiply_convert_fusion.7
  236.7 16.4 %all-to-all-done.2 = f32[32,1,1024]{2,1,0:T(1,128)S(1)} async-done(((f32[32,1,1024]{2,1,0:T(1,128)}), f32[32,1,1024]{2,1,0:T(1,128)S(1)}, u32[]{:S(2)}, u32[]{:S(2)}) %all-to-all-start.2) | async-done | bytes 131104 | tf_op jit(solution)/shard_map/all_to_all | solution.py:165
  253.2 0.9 reduce.18
  254.5 1.4 fusion.1
  255.9 2.1 fusion
  258.0 1.4 copy.186
  259.5 1.4 reshape.479
  260.9 2.2 multiply_reduce_fusion
  263.1 0.8 multiply_convert_fusion.2
  (129 shorter events, 15.2 us)
Async XLA Ops:
  0.6 1.6 copy-start
  0.6 9.3 %copy-start.2 = (bf16[2048,128]{1,0:T(8,128)(2,1)S(1)}, bf16[2048,128]{1,0:T(8,128)(2,1)}, u32[]{:S(2)}) copy-start(bf16[2048,128]{1,0:T(8,128)(2,1)} %param.19) | copy-start | bytes 1572868
  2.2 13.7 %copy-start.17 = (bf16[2048]{0:T(1024)(128)(2,1)S(1)}, bf16[2048]{0:T(1024)(128)(2,1)}, u32[]{:S(2)}) copy-start(bf16[2048]{0:T(1024)(128)(2,1)} %param.16) | copy-start | bytes 12292
  2.2 13.7 %copy-start.27 = (f32[32]{0:T(128)S(1)}, f32[32]{0:T(128)}, u32[]{:S(2)}) copy-start(f32[32]{0:T(128)} %param.26) | copy-start | bytes 388
  2.2 13.8 %copy-start.28 = (f32[32]{0:T(128)S(1)}, f32[32]{0:T(128)}, u32[]{:S(2)}) copy-start(f32[32]{0:T(128)} %param.25) | copy-start | bytes 388
  4.0 13.5 %copy-start.12 = (f32[512,4]{0,1:T(4,128)S(1)}, f32[512,4]{0,1:T(4,128)}, u32[]{:S(2)}) copy-start(f32[512,4]{0,1:T(4,128)} %param.27) | copy-start | bytes 24580
  4.6 139.3 %collective-permute-start.2 = (bf16[3,128]{1,0:T(4,128)(2,1)}, bf16[3,128]{1,0:T(4,128)(2,1)}, u32[]{:S(2)}, u32[]{:S(2)}) collective-permute-start(bf16[3,128]{1,0:T(4,128)(2,1)} %get-tuple-element.46), channel_id=1, source_target_pairs={{0,8},{8,16},{16,24},{24,32},{32,40},{40,48},{48,56},{56,64},{64,7... | collective-permute-start | bytes 2312 | tf_op jit(solution)/shard_map/ppermute | solution.py:16
  10.6 8.4 %copy-start.3 = (bf16[512,128]{1,0:T(8,128)(2,1)}, bf16[512,128]{1,0:T(8,128)(2,1)S(1)}, u32[]{:S(2)}) copy-start(bf16[512,128]{1,0:T(8,128)(2,1)S(1)} %convolution_convert_fusion.3) | copy-start | bytes 393220
  11.3 131.8 %collective-permute-start.1 = (bf16[3,128]{1,0:T(4,128)(2,1)}, bf16[3,128]{1,0:T(4,128)(2,1)}, u32[]{:S(2)}, u32[]{:S(2)}) collective-permute-start(bf16[3,128]{1,0:T(4,128)(2,1)} %get-tuple-element.44), channel_id=1, source_target_pairs={{0,8},{8,16},{16,24},{24,32},{32,40},{40,48},{48,56},{56,64},{64,7... | collective-permute-start | bytes 2312 | tf_op jit(solution)/shard_map/ppermute | solution.py:16
  19.3 51.9 %copy-start.1 = (bf16[2048,128]{1,0:T(8,128)(2,1)S(1)}, bf16[2048,128]{1,0:T(8,128)(2,1)}, u32[]{:S(2)}) copy-start(bf16[2048,128]{1,0:T(8,128)(2,1)} %param.18) | copy-start | bytes 1572868
  20.6 128.6 %all-to-all-start.1 = ((f32[32,1,1,4]{3,2,1,0:T(1,128)}), f32[32,1,1,4]{3,2,1,0:T(1,128)}, u32[]{:S(2)}, u32[]{:S(2)}) async-start(f32[32,1,1,4]{3,2,1,0:T(1,128)} %broadcast_in_dim.36), calls=%async_computation.1 | async-start | bytes 32768 | tf_op jit(solution)/shard_map/all_to_all | solution.py:32
  65.5 0.7 copy-start.6
  66.8 78.9 %collective-permute-start = (bf16[3,256]{1,0:T(4,128)(2,1)}, bf16[3,256]{1,0:T(4,128)(2,1)}, u32[]{:S(2)}, u32[]{:S(2)}) collective-permute-start(bf16[3,256]{1,0:T(4,128)(2,1)} %get-tuple-element.42), channel_id=1, source_target_pairs={{0,8},{8,16},{16,24},{24,32},{32,40},{40,48},{48,56},{56,64},{64,7... | collective-permute-start | bytes 4616 | tf_op jit(solution)/shard_map/ppermute | solution.py:16
  72.0 6.7 %copy-start.9 = (f32[4,1,1,4]{3,2,1,0:T(1,128)S(1)}, f32[4,1,1,4]{3,2,1,0:T(1,128)}, u32[]{:S(2)}) copy-start(f32[4,1,1,4]{3,2,1,0:T(1,128)} %get-tuple-element.36) | copy-start | bytes 196
  72.0 7.9 %copy-start.13 = (bf16[3,256]{1,0:T(4,128)(2,1)S(1)}, bf16[3,256]{1,0:T(4,128)(2,1)}, u32[]{:S(2)}) copy-start(bf16[3,256]{1,0:T(4,128)(2,1)} %get-tuple-element.41) | copy-start | bytes 4612
  72.0 7.9 %copy-start.18 = (bf16[3,128]{1,0:T(4,128)(2,1)S(1)}, bf16[3,128]{1,0:T(4,128)(2,1)}, u32[]{:S(2)}) copy-start(bf16[3,128]{1,0:T(4,128)(2,1)} %get-tuple-element.45) | copy-start | bytes 2308
  72.0 7.9 %copy-start.19 = (bf16[3,128]{1,0:T(4,128)(2,1)S(1)}, bf16[3,128]{1,0:T(4,128)(2,1)}, u32[]{:S(2)}) copy-start(bf16[3,128]{1,0:T(4,128)(2,1)} %get-tuple-element.43) | copy-start | bytes 2308
  72.0 64.3 %copy-start.20 = (bf16[1,128]{1,0:T(2,128)(2,1)S(1)}, bf16[1,128]{1,0:T(2,128)(2,1)}, u32[]{:S(2)}) copy-start(bf16[1,128]{1,0:T(2,128)(2,1)} %fusion.5) | copy-start | bytes 772
  72.0 65.0 %copy-start.26 = (f32[4]{0:T(128)S(1)}, f32[4]{0:T(128)}, u32[]{:S(2)}) copy-start(f32[4]{0:T(128)} %get-tuple-element.57) | copy-start | bytes 52
  72.0 71.1 %copy-start.4 = (bf16[512,128]{1,0:T(8,128)(2,1)S(1)}, bf16[512,128]{1,0:T(8,128)(2,1)}, u32[]{:S(2)}) copy-start(bf16[512,128]{1,0:T(8,128)(2,1)} %copy-done.3) | copy-start | bytes 393220
  78.6 67.2 %copy-start.7 = (bf16[512,256]{1,0:T(8,128)(2,1)S(1)}, bf16[512,256]{1,0:T(8,128)(2,1)}, u32[]{:S(2)}) copy-start(bf16[512,256]{1,0:T(8,128)(2,1)} %copy-done.6) | copy-start | bytes 786436
  143.9 2.9 %copy-start.5 = (bf16[512,128]{1,0:T(8,128)(2,1)}, bf16[512,128]{1,0:T(8,128)(2,1)S(1)}, u32[]{:S(2)}) copy-start(bf16[512,128]{1,0:T(8,128)(2,1)S(1)} %multiply_convert_fusion.6) | copy-start | bytes 393220
  146.5 1.0 copy-start.14
  146.5 1.0 copy-start.15
  146.5 1.0 copy-start.21
  146.5 1.0 copy-start.22
  146.9 46.2 %copy-start.24 = (f32[4]{0:T(128)S(1)}, f32[4]{0:T(128)}, u32[]{:S(2)}) copy-start(f32[4]{0:T(128)} %get-tuple-element.25) | copy-start | bytes 52
  146.9 46.3 %copy-start.25 = (bf16[1,128]{1,0:T(2,128)(2,1)S(1)}, bf16[1,128]{1,0:T(2,128)(2,1)}, u32[]{:S(2)}) copy-start(bf16[1,128]{1,0:T(2,128)(2,1)} %fusion.80) | copy-start | bytes 772
  147.0 52.4 %copy-start.10 = (pred[32,32]{1,0:T(8,128)(4,1)S(1)}, pred[32,32]{1,0:T(8,128)(4,1)}, u32[]{:S(2)}) copy-start(pred[32,32]{1,0:T(8,128)(4,1)} %iota_compare_fusion.1) | copy-start | bytes 3076
  149.1 43.7 %all-to-all-start = ((bf16[32,2,512]{2,1,0:T(2,128)(2,1)}), bf16[32,2,512]{2,1,0:T(2,128)(2,1)S(1)}, u32[]{:S(2)}, u32[]{:S(2)}) async-start(bf16[32,2,512]{2,1,0:T(2,128)(2,1)} %reshape.495), calls=%async_computation | async-start | bytes 131072 | tf_op jit(solution)/shard_map/all_to_all | solution.py:158
  194.1 27.7 %all-to-all-start.3 = ((f32[32,1,256]{2,1,0:T(1,128)}), f32[32,1,256]{2,1,0:T(1,128)}, u32[]{:S(2)}, u32[]{:S(2)}) async-start(f32[32,1,256]{2,1,0:T(1,128)} %reshape.499), calls=%async_computation.3 | async-start | bytes 65536 | tf_op jit(solution)/shard_map/all_to_all | solution.py:32
  200.8 55.1 %copy-start.8 = (f32[4,128,128]{2,1,0:T(8,128)S(1)}, f32[4,128,128]{2,1,0:T(8,128)}, u32[]{:S(2)}) copy-start(f32[4,128,128]{2,1,0:T(8,128)} %fusion.88) | copy-start | bytes 786436
  221.8 31.3 %all-to-all-start.2 = ((f32[32,1,1024]{2,1,0:T(1,128)}), f32[32,1,1024]{2,1,0:T(1,128)S(1)}, u32[]{:S(2)}, u32[]{:S(2)}) async-start(f32[32,1,1024]{2,1,0:T(1,128)} %reshape.497), calls=%async_computation.2 | async-start | bytes 262144 | tf_op jit(solution)/shard_map/all_to_all | solution.py:165
  229.8 26.1 %copy-start.11 = (pred[128,128]{1,0:T(8,128)(4,1)S(1)}, pred[128,128]{1,0:T(8,128)(4,1)}, u32[]{:S(2)}) copy-start(pred[128,128]{1,0:T(8,128)(4,1)} %iota_compare_fusion) | copy-start | bytes 49156
  258.0 2.9 %copy-start.23 = (f32[256]{0:T(256)S(1)}, f32[256]{0:T(256)}, u32[]{:S(2)}) copy-start(f32[256]{0:T(256)} %mul.534) | copy-start | bytes 3076
  260.9 2.2 copy-start.16
where the time goes:
time: 265 us; the launch traced here: 264 us
  starting transfers between devices  86.9 us (33%)
  waiting for transfers between devices  59.6 us (22%)
  blocking collectives  56.4 us (21%)
  other arithmetic  21.9 us (8%)
  matrix products  19.2 us (7%)
  local copies, waits for them, and re-layouts  18 us (7%)
    psum x1, blocking collectives, from_root(): return lax.psum(kept, axis)  56.4 us
    all_to_all x2, starting transfers between devices, from_everyone(): lax.all_to_all(jnp.broadcast_to(value[None], (peers, *value.shape)), axis...  48.4 us
    all_to_all x1, waiting for transfers between devices, on_device(): lax.all_to_all(running[None], 'sp', split_axis=1, concat_axis=0, tiled=True)  22.1 us
    all_to_all x2, waiting for transfers between devices, from_everyone(): lax.all_to_all(jnp.broadcast_to(value[None], (peers, *value.shape)), axis...  21.1 us
    all_to_all x1, starting transfers between devices, on_device(): lax.all_to_all(running[None], 'sp', split_axis=1, concat_axis=0, tiled=True)  19.8 us
    all_to_all x1, waiting for transfers between devices, on_device(): lax.all_to_all(prefix_rows, 'sp', split_axis=0, concat_axis=1, tiled=True)  16.4 us
    ppermute x3, starting transfers between devices, passed_along(): return lax.ppermute(block, axis, route)  13.8 us
    dot_general x8, matrix products, project(): jnp.dot(operand, weights, preferred_element_type=jnp.float32)  11.1 us
  transfers between devices with their start and end apart: 7, of which 3 were waited for; matrix products, arithmetic and copies ran while one was open for 16% of the time, Pallas kernels for 0%

commit v1 on v0

--- a/solution.py
+++ b/solution.py
@@ -18,7 +18,7 @@
 
 def from_root(value, axis, source):
     kept = jnp.where(lax.axis_index(axis) == source, value, 0).astype(value.dtype)
-    return lax.psum(kept, axis)
+    return lax.all_gather(kept, axis).sum(axis=0)
 
 
 def in_order(pieces, dim):

time: 265 us -> 370 us (1.40)
  blocking collectives: 56.4 us -> 161 us
    all_gather x0 -> x3, blocking collectives: none -> 161 us  [from_root(): return lax.all_gather(kept, axis).sum(axis=0)]
    psum x1 -> x0, blocking collectives: 56.4 us -> none  [from_root(): return lax.psum(kept, axis)]
  transfers between devices with their start and end apart: 7 -> 7, of which waited for: 3 -> 3; matrix products, arithmetic and copies ran while one was open for 16% -> 12% of each run, Pallas kernels for 0% -> 0%
where the time goes in v1:
time: 370 us; the launch traced here: 369 us
  blocking collectives  161 us (44%)
  starting transfers between devices  86 us (23%)
  waiting for transfers between devices  59.8 us (16%)
  other arithmetic  22 us (6%)
  matrix products  19.1 us (5%)
  local copies, waits for them, and re-layouts  18.7 us (5%)
    all_gather x3, blocking collectives, from_root(): return lax.all_gather(kept, axis).sum(axis=0)  161 us
    all_to_all x2, starting transfers between devices, from_everyone(): lax.all_to_all(jnp.broadcast_to(value[None], (peers, *value.shape)), axis...  48.4 us
    all_to_all x1, waiting for transfers between devices, on_device(): lax.all_to_all(running[None], 'sp', split_axis=1, concat_axis=0, tiled=True)  22.1 us
    all_to_all x2, waiting for transfers between devices, from_everyone(): lax.all_to_all(jnp.broadcast_to(value[None], (peers, *value.shape)), axis...  21.1 us
    all_to_all x1, starting transfers between devices, on_device(): lax.all_to_all(running[None], 'sp', split_axis=1, concat_axis=0, tiled=True)  18.9 us
    all_to_all x1, waiting for transfers between devices, on_device(): lax.all_to_all(prefix_rows, 'sp', split_axis=0, concat_axis=1, tiled=True)  16.6 us
    ppermute x3, starting transfers between devices, passed_along(): return lax.ppermute(block, axis, route)  13.8 us
    dot_general x8, matrix products, project(): jnp.dot(operand, weights, preferred_element_type=jnp.float32)  11.1 us
  transfers between devices with their start and end apart: 7, of which 3 were waited for; matrix products, arithmetic and copies ran while one was open for 12% of the time, Pallas kernels for 0%

profile of v1, /device:TPU:46, one launch (start us, length us, event | category | flops | bytes accessed | tf_op | source)
XLA Modules:
  0.0 368.7 jit_solution(13538097520180829)
XLA Ops:
  0.7 1.6 copy-done
  2.2 1.8 convolution_convert_fusion.2
  4.6 5.2 %collective-permute-start.2 = (bf16[3,128]{1,0:T(4,128)(2,1)}, bf16[3,128]{1,0:T(4,128)(2,1)}, u32[]{:S(2)}, u32[]{:S(2)}) collective-permute-start(bf16[3,128]{1,0:T(4,128)(2,1)} %get-tuple-element.43), channel_id=1, source_target_pairs={{0,8},{8,16},{16,24},{24,32},{32,40},{40,48},{48,56},{56,64},{64,7... | collective-permute-start | bytes 2312 | tf_op jit(solution)/shard_map/ppermute | solution.py:16
  9.9 0.7 convolution_convert_fusion.3
  11.2 4.7 %collective-permute-start.1 = (bf16[3,128]{1,0:T(4,128)(2,1)}, bf16[3,128]{1,0:T(4,128)(2,1)}, u32[]{:S(2)}, u32[]{:S(2)}) collective-permute-start(bf16[3,128]{1,0:T(4,128)(2,1)} %get-tuple-element.41), channel_id=1, source_target_pairs={{0,8},{8,16},{16,24},{24,32},{32,40},{40,48},{48,56},{56,64},{64,7... | collective-permute-start | bytes 2312 | tf_op jit(solution)/shard_map/ppermute | solution.py:16
  16.1 1.4 multiply_exponential_fusion
  17.5 1.4 multiply_subtract_fusion
  20.5 43.0 %all-to-all-start.1 = ((f32[32,1,1,4]{3,2,1,0:T(1,128)}), f32[32,1,1,4]{3,2,1,0:T(1,128)}, u32[]{:S(2)}, u32[]{:S(2)}) async-start(f32[32,1,1,4]{3,2,1,0:T(1,128)} %broadcast_in_dim.36), calls=%async_computation.1 | async-start | bytes 32768 | tf_op jit(solution)/shard_map/all_to_all | solution.py:32
  63.5 1.9 convolution_convert_fusion.1
  65.4 0.7 copy-done.6
  66.7 3.8 %collective-permute-start = (bf16[3,256]{1,0:T(4,128)(2,1)}, bf16[3,256]{1,0:T(4,128)(2,1)}, u32[]{:S(2)}, u32[]{:S(2)}) collective-permute-start(bf16[3,256]{1,0:T(4,128)(2,1)} %get-tuple-element.39), channel_id=1, source_target_pairs={{0,8},{8,16},{16,24},{24,32},{32,40},{40,48},{48,56},{56,64},{64,7... | collective-permute-start | bytes 4616 | tf_op jit(solution)/shard_map/ppermute | solution.py:16
  71.2 0.7 fusion.5
  72.1 1.5 fusion.89
  74.9 0.7 dynamic_slice.39
  75.6 0.7 constant_dynamic-slice_fusion.4
  77.1 2.0 fusion.90
  79.2 54.9 %all-gather.4 = bf16[32,3,128]{2,1,0:T(4,128)(2,1)S(1)} all-gather(bf16[1,3,128]{2,1,0:T(4,128)(2,1)S(1)} %copy-done.19), channel_id=3, replica_groups=mesh['grp'=2,'sp'=32,'tp'=8] {'sp'}, dimensions={0}, use_global_device_ids=true | all-gather | bytes 25344 | tf_op jit(solution)/shard_map/all_gather | solution.py:21
  134.2 52.2 %all-gather.3 = bf16[32,3,128]{2,1,0:T(4,128)(2,1)S(1)} all-gather(bf16[1,3,128]{2,1,0:T(4,128)(2,1)S(1)} %copy-done.18), channel_id=2, replica_groups=mesh['grp'=2,'sp'=32,'tp'=8] {'sp'}, dimensions={0}, use_global_device_ids=true | all-gather | bytes 25344 | tf_op jit(solution)/shard_map/all_gather | solution.py:21
  188.2 54.1 %all-gather.5 = bf16[32,3,256]{2,1,0:T(4,128)(2,1)S(1)} all-gather(bf16[1,3,256]{2,1,0:T(4,128)(2,1)S(1)} %copy-done.13), channel_id=4, replica_groups=mesh['grp'=2,'sp'=32,'tp'=8] {'sp'}, dimensions={0}, use_global_device_ids=true | all-gather | bytes 50688 | tf_op jit(solution)/shard_map/all_gather | solution.py:21
  243.1 2.2 fusion.85
  247.2 0.7 copy.147
  249.5 0.7 maximum_convert_fusion.2
  250.3 0.9 fusion.88
  251.2 0.7 maximum_convert_fusion
  253.0 0.8 slice_add_fusion
  253.9 0.8 reshape.507
  254.6 18.9 %all-to-all-start = ((bf16[32,2,512]{2,1,0:T(2,128)(2,1)}), bf16[32,2,512]{2,1,0:T(2,128)(2,1)S(1)}, u32[]{:S(2)}, u32[]{:S(2)}) async-start(bf16[32,2,512]{2,1,0:T(2,128)(2,1)} %reshape.507), calls=%async_computation | async-start | bytes 131072 | tf_op jit(solution)/shard_map/all_to_all | solution.py:158
  273.5 0.8 fusion.48
  274.3 0.8 copy.162
  275.2 22.1 %all-to-all-done = bf16[32,2,512]{2,1,0:T(2,128)(2,1)S(1)} async-done(((bf16[32,2,512]{2,1,0:T(2,128)(2,1)}), bf16[32,2,512]{2,1,0:T(2,128)(2,1)S(1)}, u32[]{:S(2)}, u32[]{:S(2)}) %all-to-all-start) | async-done | bytes 65568 | tf_op jit(solution)/shard_map/all_to_all | solution.py:158
  297.9 0.7 reshape.511
  298.6 5.3 %all-to-all-start.3 = ((f32[32,1,256]{2,1,0:T(1,128)}), f32[32,1,256]{2,1,0:T(1,128)}, u32[]{:S(2)}, u32[]{:S(2)}) async-start(f32[32,1,256]{2,1,0:T(1,128)} %reshape.511), calls=%async_computation.3 | async-start | bytes 65536 | tf_op jit(solution)/shard_map/all_to_all | solution.py:32
  304.4 0.9 reshape.509
  305.3 21.1 %all-to-all-done.3 = f32[32,1,256]{2,1,0:T(1,128)} async-done(((f32[32,1,256]{2,1,0:T(1,128)}), f32[32,1,256]{2,1,0:T(1,128)}, u32[]{:S(2)}, u32[]{:S(2)}) %all-to-all-start.3) | async-done | bytes 32800 | tf_op jit(solution)/shard_map/all_to_all | solution.py:32
  326.4 5.0 %all-to-all-start.2 = ((f32[32,1,1024]{2,1,0:T(1,128)}), f32[32,1,1024]{2,1,0:T(1,128)S(1)}, u32[]{:S(2)}, u32[]{:S(2)}) async-start(f32[32,1,1024]{2,1,0:T(1,128)} %reshape.509), calls=%async_computation.2 | async-start | bytes 262144 | tf_op jit(solution)/shard_map/all_to_all | solution.py:165
  331.4 1.4 fusion.39
  332.7 1.6 fusion.52
  335.6 1.5 reduce.25
  337.2 1.3 multiply_reduce_fusion.1
  339.2 1.3 multiply_convert_fusion.7
  341.3 16.6 %all-to-all-done.2 = f32[32,1,1024]{2,1,0:T(1,128)S(1)} async-done(((f32[32,1,1024]{2,1,0:T(1,128)}), f32[32,1,1024]{2,1,0:T(1,128)S(1)}, u32[]{:S(2)}, u32[]{:S(2)}) %all-to-all-start.2) | async-done | bytes 131104 | tf_op jit(solution)/shard_map/all_to_all | solution.py:165
  357.9 0.9 reduce.24
  359.2 1.4 fusion.1
  360.6 2.1 fusion
  362.7 1.4 copy.186
  364.2 1.4 reshape.491
  365.6 2.2 multiply_reduce_fusion
  367.8 0.8 multiply_convert_fusion.2
  (135 shorter events, 17.3 us)
Async XLA Ops:
  0.6 1.6 copy-start
  0.6 9.2 %copy-start.2 = (bf16[2048,128]{1,0:T(8,128)(2,1)S(1)}, bf16[2048,128]{1,0:T(8,128)(2,1)}, u32[]{:S(2)}) copy-start(bf16[2048,128]{1,0:T(8,128)(2,1)} %param.19) | copy-start | bytes 1572868
  2.2 13.7 %copy-start.17 = (bf16[2048]{0:T(1024)(128)(2,1)S(1)}, bf16[2048]{0:T(1024)(128)(2,1)}, u32[]{:S(2)}) copy-start(bf16[2048]{0:T(1024)(128)(2,1)} %param.16) | copy-start | bytes 12292
  2.2 13.7 %copy-start.27 = (f32[32]{0:T(128)S(1)}, f32[32]{0:T(128)}, u32[]{:S(2)}) copy-start(f32[32]{0:T(128)} %param.26) | copy-start | bytes 388
  2.2 13.8 %copy-start.28 = (f32[32]{0:T(128)S(1)}, f32[32]{0:T(128)}, u32[]{:S(2)}) copy-start(f32[32]{0:T(128)} %param.25) | copy-start | bytes 388
  4.0 13.5 %copy-start.12 = (f32[512,4]{0,1:T(4,128)S(1)}, f32[512,4]{0,1:T(4,128)}, u32[]{:S(2)}) copy-start(f32[512,4]{0,1:T(4,128)} %param.27) | copy-start | bytes 24580
  4.6 244.8 %collective-permute-start.2 = (bf16[3,128]{1,0:T(4,128)(2,1)}, bf16[3,128]{1,0:T(4,128)(2,1)}, u32[]{:S(2)}, u32[]{:S(2)}) collective-permute-start(bf16[3,128]{1,0:T(4,128)(2,1)} %get-tuple-element.43), channel_id=1, source_target_pairs={{0,8},{8,16},{16,24},{24,32},{32,40},{40,48},{48,56},{56,64},{64,7... | collective-permute-start | bytes 2312 | tf_op jit(solution)/shard_map/ppermute | solution.py:16
  10.6 8.3 %copy-start.3 = (bf16[512,128]{1,0:T(8,128)(2,1)}, bf16[512,128]{1,0:T(8,128)(2,1)S(1)}, u32[]{:S(2)}) copy-start(bf16[512,128]{1,0:T(8,128)(2,1)S(1)} %convolution_convert_fusion.3) | copy-start | bytes 393220
  11.2 237.4 %collective-permute-start.1 = (bf16[3,128]{1,0:T(4,128)(2,1)}, bf16[3,128]{1,0:T(4,128)(2,1)}, u32[]{:S(2)}, u32[]{:S(2)}) collective-permute-start(bf16[3,128]{1,0:T(4,128)(2,1)} %get-tuple-element.41), channel_id=1, source_target_pairs={{0,8},{8,16},{16,24},{24,32},{32,40},{40,48},{48,56},{56,64},{64,7... | collective-permute-start | bytes 2312 | tf_op jit(solution)/shard_map/ppermute | solution.py:16
  19.3 51.9 %copy-start.1 = (bf16[2048,128]{1,0:T(8,128)(2,1)S(1)}, bf16[2048,128]{1,0:T(8,128)(2,1)}, u32[]{:S(2)}) copy-start(bf16[2048,128]{1,0:T(8,128)(2,1)} %param.18) | copy-start | bytes 1572868
  20.5 234.2 %all-to-all-start.1 = ((f32[32,1,1,4]{3,2,1,0:T(1,128)}), f32[32,1,1,4]{3,2,1,0:T(1,128)}, u32[]{:S(2)}, u32[]{:S(2)}) async-start(f32[32,1,1,4]{3,2,1,0:T(1,128)} %broadcast_in_dim.36), calls=%async_computation.1 | async-start | bytes 32768 | tf_op jit(solution)/shard_map/all_to_all | solution.py:32
  65.4 0.7 copy-start.6
  66.7 184.5 %collective-permute-start = (bf16[3,256]{1,0:T(4,128)(2,1)}, bf16[3,256]{1,0:T(4,128)(2,1)}, u32[]{:S(2)}, u32[]{:S(2)}) collective-permute-start(bf16[3,256]{1,0:T(4,128)(2,1)} %get-tuple-element.39), channel_id=1, source_target_pairs={{0,8},{8,16},{16,24},{24,32},{32,40},{40,48},{48,56},{56,64},{64,7... | collective-permute-start | bytes 4616 | tf_op jit(solution)/shard_map/ppermute | solution.py:16
  71.9 7.3 %copy-start.19 = (bf16[1,3,128]{2,1,0:T(4,128)(2,1)S(1)}, bf16[1,3,128]{2,1,0:T(4,128)(2,1)}, u32[]{:S(2)}) copy-start(bf16[1,3,128]{2,1,0:T(4,128)(2,1)} %get-tuple-element.42) | copy-start | bytes 2308
  71.9 62.3 %copy-start.20 = (bf16[1,128]{1,0:T(2,128)(2,1)S(1)}, bf16[1,128]{1,0:T(2,128)(2,1)}, u32[]{:S(2)}) copy-start(bf16[1,128]{1,0:T(2,128)(2,1)} %fusion.5) | copy-start | bytes 772
  71.9 62.3 %copy-start.18 = (bf16[1,3,128]{2,1,0:T(4,128)(2,1)S(1)}, bf16[1,3,128]{2,1,0:T(4,128)(2,1)}, u32[]{:S(2)}) copy-start(bf16[1,3,128]{2,1,0:T(4,128)(2,1)} %get-tuple-element.40) | copy-start | bytes 2308
  71.9 115.1 %copy-start.9 = (f32[4,1,1,4]{3,2,1,0:T(1,128)S(1)}, f32[4,1,1,4]{3,2,1,0:T(1,128)}, u32[]{:S(2)}) copy-start(f32[4,1,1,4]{3,2,1,0:T(1,128)} %get-tuple-element.33) | copy-start | bytes 196
  71.9 116.3 %copy-start.13 = (bf16[1,3,256]{2,1,0:T(4,128)(2,1)S(1)}, bf16[1,3,256]{2,1,0:T(4,128)(2,1)}, u32[]{:S(2)}) copy-start(bf16[1,3,256]{2,1,0:T(4,128)(2,1)} %get-tuple-element.38) | copy-start | bytes 4612
  71.9 170.6 %copy-start.26 = (f32[4]{0:T(128)S(1)}, f32[4]{0:T(128)}, u32[]{:S(2)}) copy-start(f32[4]{0:T(128)} %get-tuple-element.54) | copy-start | bytes 52
  71.9 176.7 %copy-start.4 = (bf16[512,128]{1,0:T(8,128)(2,1)S(1)}, bf16[512,128]{1,0:T(8,128)(2,1)}, u32[]{:S(2)}) copy-start(bf16[512,128]{1,0:T(8,128)(2,1)} %copy-done.3) | copy-start | bytes 393220
  188.2 63.0 %copy-start.7 = (bf16[512,256]{1,0:T(8,128)(2,1)S(1)}, bf16[512,256]{1,0:T(8,128)(2,1)}, u32[]{:S(2)}) copy-start(bf16[512,256]{1,0:T(8,128)(2,1)} %copy-done.6) | copy-start | bytes 786436
  249.4 2.9 copy-start.5
  252.0 1.0 copy-start.14
  252.0 1.0 copy-start.15
  252.0 1.0 copy-start.21
  252.0 1.0 copy-start.22
  252.4 45.3 %copy-start.24 = (f32[4]{0:T(128)S(1)}, f32[4]{0:T(128)}, u32[]{:S(2)}) copy-start(f32[4]{0:T(128)} %get-tuple-element.22) | copy-start | bytes 52
  252.4 45.4 %copy-start.25 = (bf16[1,128]{1,0:T(2,128)(2,1)S(1)}, bf16[1,128]{1,0:T(2,128)(2,1)}, u32[]{:S(2)}) copy-start(bf16[1,128]{1,0:T(2,128)(2,1)} %fusion.80) | copy-start | bytes 772
  252.5 51.5 %copy-start.10 = (pred[32,32]{1,0:T(8,128)(4,1)S(1)}, pred[32,32]{1,0:T(8,128)(4,1)}, u32[]{:S(2)}) copy-start(pred[32,32]{1,0:T(8,128)(4,1)} %iota_compare_fusion.1) | copy-start | bytes 3076
  254.6 42.7 %all-to-all-start = ((bf16[32,2,512]{2,1,0:T(2,128)(2,1)}), bf16[32,2,512]{2,1,0:T(2,128)(2,1)S(1)}, u32[]{:S(2)}, u32[]{:S(2)}) async-start(bf16[32,2,512]{2,1,0:T(2,128)(2,1)} %reshape.507), calls=%async_computation | async-start | bytes 131072 | tf_op jit(solution)/shard_map/all_to_all | solution.py:158
  298.6 27.8 %all-to-all-start.3 = ((f32[32,1,256]{2,1,0:T(1,128)}), f32[32,1,256]{2,1,0:T(1,128)}, u32[]{:S(2)}, u32[]{:S(2)}) async-start(f32[32,1,256]{2,1,0:T(1,128)} %reshape.511), calls=%async_computation.3 | async-start | bytes 65536 | tf_op jit(solution)/shard_map/all_to_all | solution.py:32
  305.3 55.3 %copy-start.8 = (f32[4,128,128]{2,1,0:T(8,128)S(1)}, f32[4,128,128]{2,1,0:T(8,128)}, u32[]{:S(2)}) copy-start(f32[4,128,128]{2,1,0:T(8,128)} %fusion.88) | copy-start | bytes 786436
  326.4 31.5 %all-to-all-start.2 = ((f32[32,1,1024]{2,1,0:T(1,128)}), f32[32,1,1024]{2,1,0:T(1,128)S(1)}, u32[]{:S(2)}, u32[]{:S(2)}) async-start(f32[32,1,1024]{2,1,0:T(1,128)} %reshape.509), calls=%async_computation.2 | async-start | bytes 262144 | tf_op jit(solution)/shard_map/all_to_all | solution.py:165
  334.4 26.2 %copy-start.11 = (pred[128,128]{1,0:T(8,128)(4,1)S(1)}, pred[128,128]{1,0:T(8,128)(4,1)}, u32[]{:S(2)}) copy-start(pred[128,128]{1,0:T(8,128)(4,1)} %iota_compare_fusion) | copy-start | bytes 49156
  362.7 2.9 copy-start.23
  365.6 2.2 copy-start.16
